TPU v7x, 512 devices: a 8x2x16 block of a 8x16x16 slice. The times are simulated.
512 devices in a mesh: grp: 2 (over y), fs: 16 (over z), tp: 16 (over x, core).
Axes of the slice: x: 8, y: 2, z: 16, core: 2. Of those that a mesh axis runs over, the one named last changes fastest.
The devices are a block of a 8x16x16 slice.
Arguments:
- tokens: bfloat16 [16384, 2048], P(('grp', 'fs')), parts along dimension 0, may hold values from -6 to 6
- pre_gain: float32 [2048], replicated, may hold values from 0.1 to 1.9
- gate_weight: float32 [2048, 5632], P('fs', 'tp'), may hold values from -0.125 to 0.125
- gate_scale: float32 [5632], P('tp'), may hold values from 0.5 to 2
- up_weight: float32 [2048, 5632], P('fs', 'tp'), may hold values from -0.125 to 0.125
- up_scale: float32 [5632], P('tp'), may hold values from 0.5 to 2
- down_weight: float32 [5632, 2048], P('tp', 'fs'), may hold values from -0.078125 to 0.078125
- down_scale: float32 [2048], replicated, may hold values from 0.3 to 3
- post_gain: float32 [2048], replicated, may hold values from 0.1 to 1.9
Outputs:
- mixed: bfloat16 [16384, 2048], P(('grp', 'fs')), parts along dimension 0
There are 2 independent parts, one for each index of `grp`. A program takes and returns all parts, laid end to end along the dimension named above; an argument that names none is the same for every part. Nothing has to cross between parts.
All inputs are finite; a program needn't handle non-finite values.
Results may differ from a plain program's by a relative error of at most 0.018.
Values may be sent and summed in bfloat16 or wider, within the bound.
No kernel may reach another device: no remote copies, remote signals or barrier semaphores. Data moves between devices by JAX's collectives and lax.ppermute only.
A program may use at most 64 MiB of HBM per device.

v0:
```python
import jax
import jax.numpy as jnp
from jax import lax
from jax.sharding import PartitionSpec as P

EPS = 1e-06


def side_by_side(arrays, axis, dim, along):
    ends, at = ([], 0)
    for a in arrays[:-1]:
        at += a.shape[along]
        ends.append(at)
    both = jnp.concatenate(arrays, axis=along)
    return tuple(jnp.split(lax.all_gather(both, axis, axis=dim, tiled=True), ends, axis=along))


def from_everyone(array, axis):
    copies = jnp.broadcast_to(array, (lax.axis_size(axis), *array.shape))
    return lax.all_to_all(copies, axis, split_axis=0, concat_axis=0, tiled=True)


def joined_along(parts, dim):
    lengths = list(parts.shape[1:])
    lengths[dim] *= parts.shape[0]
    return jnp.moveaxis(parts, 0, dim).reshape(lengths)


def collect(array, axis, dim):
    parts = from_everyone(array, axis)
    return joined_along(parts, dim)


def cut_along(array, dim, count):
    lengths = array.shape
    parts = array.reshape(*lengths[:dim], count, lengths[dim] // count, *lengths[dim + 1 :])
    return jnp.moveaxis(parts, dim, 0)


def sent_and_summed(array, axis, dim):
    count = lax.axis_size(axis)
    parts = lax.all_to_all(cut_along(array, dim, count), axis, 0, 0, tiled=True)
    return jnp.sum(parts.astype(jnp.float32), axis=0)


def finish(summed, down_scale, post_gain):
    branch = summed * down_scale
    return (
        branch * lax.rsqrt(jnp.mean(branch * branch, axis=-1, keepdims=True) + EPS) * post_gain
    ).astype(jnp.bfloat16)


def body(
    tokens,
    pre_gain,
    gate_weight,
    gate_scale,
    up_weight,
    up_scale,
    down_weight,
    down_scale,
    post_gain,
):
    rows = tokens.astype(jnp.float32)
    normed = (
        rows * lax.rsqrt(jnp.mean(rows * rows, axis=-1, keepdims=True) + EPS) * pre_gain
    ).astype(jnp.bfloat16)
    gate_low = gate_weight.astype(jnp.bfloat16)
    up_low = up_weight.astype(jnp.bfloat16)
    down_low = down_weight.astype(jnp.bfloat16)
    gate_full, up_full = side_by_side((gate_low, up_low), "fs", 0, 1)
    gate = jnp.dot(normed, gate_full, preferred_element_type=jnp.float32) * gate_scale
    up = jnp.dot(normed, up_full, preferred_element_type=jnp.float32) * up_scale
    hidden = (jax.nn.silu(gate) * up).astype(jnp.bfloat16)
    down_full = collect(down_low, "fs", 1)
    summed = sent_and_summed(
        jnp.dot(hidden, down_full, preferred_element_type=jnp.float32).astype(jnp.bfloat16), "tp", 0
    )
    scaled = finish(summed, down_scale, post_gain)
    return lax.all_gather(scaled, "tp", axis=0, tiled=True)


def solution(mesh):
    in_specs = (
        P(("grp", "fs"), None),
        P(),
        P("fs", "tp"),
        P("tp"),
        P("fs", "tp"),
        P("tp"),
        P("tp", "fs"),
        P(),
        P(),
    )
    out_specs = P(("grp", "fs"), None)
    return jax.shard_map(body, mesh=mesh, in_specs=in_specs, out_specs=out_specs, check_vma=False)
```

profile of v0, /device:TPU:65, one launch (start us, length us, event | category | flops | bytes accessed | tf_op | source)
XLA Modules:
  0.0 292.3 jit_solution(8846115028078084117)
XLA Ops:
  6.5 0.0 all-gather.3.cloned.1.call-start
  6.6 0.9 convert_element_type.29
  7.5 0.9 convert_element_type.30
  8.4 0.7 pad_maximum_fusion
  9.1 0.1 all-gather.3.cloned.1.call-update
  9.2 0.9 convert_element_type.32
  10.1 0.0 copy-start
  10.1 1.3 broadcast_in_dim.2
  11.4 44.4 %all-to-all-start = ((bf16[16,352,128]{2,1,0:T(8,128)(2,1)}), bf16[16,352,128]{2,1,0:T(8,128)(2,1)S(1)}, u32[]{:S(2)}, u32[]{:S(2)}) async-start(bf16[16,352,128]{2,1,0:T(8,128)(2,1)} %broadcast_in_dim.2), calls=%async_computation | async-start | bytes 2883584 | tf_op jit(solution)/shard_map/all_to_all | solution.py:20
  55.8 0.1 all-gather.5.cloned.1.call-start
  55.9 0.0 copy-done
  55.9 0.5 fusion
  56.4 111.5 %all-gather.3.cloned.1.call-done = bf16[2048,704]{0,1:T(8,128)(2,1)} async-done(((bf16[128,704]{0,1:T(8,128)(2,1)}), bf16[2048,704]{0,1:T(8,128)(2,1)}) %all-gather.3.cloned.1.call-update) | async-done | bytes 2883600 | tf_op jit(solution)/shard_map/all_gather | solution.py:15
  167.8 3.2 %fusion.9 = f32[512,352]{0,1:T(8,128)} fusion(bf16[2048,704]{0,1:T(8,128)(2,1)} %all-gather.3.cloned.1.call-done, bf16[512,2048]{1,0:T(8,128)(2,1)S(1)} %copy-done, f32[2048]{0:T(1024)S(1)} %copy-done.3, f32[512]{0:T(512)S(1)} %add_rsqrt_fusion, f32[352]{0:T(512)S(1)} %copy-done.4), kind=kOutput, calls=%fused_computation.13 | convolution fusion | flops 742572032 | bytes 4271488 | tf_op jit(solution)/shard_map/dot_general | solution.py:72
  171.1 0.0 all-to-all-done
  171.1 5.2 %convolution_convert_fusion = bf16[512,2048]{1,0:T(8,128)(2,1)} fusion(bf16[2048,704]{0,1:T(8,128)(2,1)} %all-gather.3.cloned.1.call-done, f32[512,352]{0,1:T(8,128)} %fusion.9, bf16[512,2048]{1,0:T(8,128)(2,1)S(1)} %copy-done, f32[2048]{0:T(1024)S(1)} %copy-done.3, f32[512]{0:T(512)S(1)} %add_rsqrt_fusion, f32[352]{0:T(512)} %param.14, ...), kind=kOutput, calls=%fused_computation.6 | convolution fusion | flops 1482899456 | bytes 7811072 | tf_op jit(solution)/shard_map/dot_general | solution.py:77
  176.3 67.1 %all_to_all.10 = bf16[16,32,2048]{2,1,0:T(8,128)(2,1)S(1)} all-to-all(bf16[16,32,2048]{2,1,0:T(8,128)(2,1)} %bitcast.9), channel_id=1, replica_groups=mesh['grp'=2,'fs'=16,'tp'=16] {'tp'}, dimensions={0} | all-to-all | bytes 4194304 | tf_op jit(solution)/shard_map/all_to_all | solution.py:42
  243.4 0.4 convert_reduce_fusion
  243.8 0.3 copy-done.1
  244.1 0.1 multiply_reduce_fusion
  244.3 0.8 multiply_convert_fusion
  245.0 0.1 all-gather.5.cloned.1.call-update
  245.1 37.2 %all-gather.5.cloned.1.call-done = bf16[512,2048]{1,0:T(8,128)(2,1)} async-done(((bf16[32,2048]{1,0:T(8,128)(2,1)}), bf16[512,2048]{1,0:T(8,128)(2,1)}) %all-gather.5.cloned.1.call-update) | async-done | bytes 2097168 | tf_op jit(solution)/shard_map/all_gather | solution.py:80
  282.3 3.2 %copy.17 = bf16[512,2048]{1,0:T(8,128)(2,1)} copy(bf16[512,2048]{1,0:T(8,128)(2,1)} %all-gather.5.cloned.1.call-done) | data formatting | bytes 4194304
  (9 shorter events, 0.0 us)
Async XLA Ops:
  6.5 161.3 %all-gather.3.cloned.1.call-start = ((), (), s32[]{:S(2)}) async-start(), calls=%async_computation.2 | async-start | bytes 3063808 | tf_op jit(solution)/shard_map/all_gather | solution.py:15
  10.1 45.7 %copy-start = (bf16[512,2048]{1,0:T(8,128)(2,1)S(1)}, bf16[512,2048]{1,0:T(8,128)(2,1)}, u32[]{:S(2)}) copy-start(bf16[512,2048]{1,0:T(8,128)(2,1)} %param.9) | copy-start | bytes 6291460
  11.4 156.4 %copy-start.3 = (f32[2048]{0:T(1024)S(1)}, f32[2048]{0:T(1024)}, u32[]{:S(2)}) copy-start(f32[2048]{0:T(1024)} %param.10) | copy-start | bytes 24580
  11.4 156.4 %copy-start.4 = (f32[352]{0:T(512)S(1)}, f32[352]{0:T(512)}, u32[]{:S(2)}) copy-start(f32[352]{0:T(512)} %param.12) | copy-start | bytes 4228
  11.4 159.7 %all-to-all-start = ((bf16[16,352,128]{2,1,0:T(8,128)(2,1)}), bf16[16,352,128]{2,1,0:T(8,128)(2,1)S(1)}, u32[]{:S(2)}, u32[]{:S(2)}) async-start(bf16[16,352,128]{2,1,0:T(8,128)(2,1)} %broadcast_in_dim.2), calls=%async_computation | async-start | bytes 2883584 | tf_op jit(solution)/shard_map/all_to_all | solution.py:20
  55.8 226.5 %all-gather.5.cloned.1.call-start = ((), (), s32[]{:S(2)}) async-start(), calls=%async_computation.3 | async-start | bytes 2228224 | tf_op jit(solution)/shard_map/all_gather | solution.py:80
  243.4 0.7 copy-start.1
  243.4 0.8 copy-start.2
Sparse Core Ops, SparseCore 0:
  9.4 158.4 all-gather.2
  245.2 37.0 all-gather.4
where the time goes:
time: 293 us; the launch traced here: 292 us
  waiting for transfers between devices  149 us (51%)
  blocking collectives  67.1 us (23%)
  starting transfers between devices  44.4 us (15%)
  between operations  13.5 us (5%)
  matrix products  8.45 us (3%)
  other arithmetic  5.27 us (2%)
  local copies, waits for them, and re-layouts  4.77 us (2%)
    all_gather x1, waiting for transfers between devices, side_by_side(): lax.all_gather(both, axis, axis=dim, tiled=True)  111 us
    all_to_all x1, blocking collectives, sent_and_summed(): parts = lax.all_to_all(cut_along(array, dim, count), axis, 0, 0, tiled=True)  67.1 us
    all_to_all x1, starting transfers between devices, from_everyone(): return lax.all_to_all(copies, axis, split_axis=0, concat_axis=0, tiled=True)  44.4 us
    all_gather x1, waiting for transfers between devices, body(): return lax.all_gather(scaled, 'tp', axis=0, tiled=True)  37.2 us
  transfers between devices with their start and end apart: 3, of which 2 were waited for; matrix products, arithmetic and copies ran while one was open for 2% of the time, Pallas kernels for 0%

commit v1 on v0

--- a/solution.py
+++ b/solution.py
@@ -4,6 +4,28 @@
 from jax.sharding import PartitionSpec as P
 
 EPS = 1e-06
+
+
+def in_order(tiles, dim):
+    tiles = jnp.moveaxis(tiles, 0, dim)
+    shape = tiles.shape
+    return tiles.reshape(*shape[:dim], shape[dim] * shape[dim + 1], *shape[dim + 2 :])
+
+
+def collect_2(x, axis, dim):
+    size = lax.axis_size(axis)
+    pairs = [(i, (i + 1) % size) for i in range(size)]
+    back = [(b, a) for a, b in pairs]
+    lower, upper = ([], [])
+    for step in range(size - 1):
+        if step % 2 == 0:
+            lower.append(lax.ppermute(lower[-1] if lower else x, axis, pairs))
+        else:
+            upper.append(lax.ppermute(upper[-1] if upper else x, axis, back))
+    blocks = jnp.stack([*lower[::-1], x, *upper])
+    shift = lax.axis_index(axis) - len(lower)
+    blocks = blocks[(jnp.arange(size) - shift) % size]
+    return in_order(blocks, dim)
 
 
 def side_by_side(arrays, axis, dim, along):
@@ -77,7 +99,7 @@
         jnp.dot(hidden, down_full, preferred_element_type=jnp.float32).astype(jnp.bfloat16), "tp", 0
     )
     scaled = finish(summed, down_scale, post_gain)
-    return lax.all_gather(scaled, "tp", axis=0, tiled=True)
+    return collect_2(scaled, "tp", 0)
 
 
 def solution(mesh):

time: 293 us -> 298 us (1.017)
  starting transfers between devices: 44.4 us -> 72.8 us
  waiting for transfers between devices: 149 us -> 121 us
    all_gather x1 -> x0, waiting for transfers between devices: 37.2 us -> none  [body(): return lax.all_gather(scaled, 'tp', axis=0, tiled=True)]
    ppermute x0 -> x15, starting transfers between devices: none -> 28.4 us  [the longest x7 20.1 us: collect_2(): upper.append(lax.ppermute(upper[-1] if upper else x, axis, back))]
    ppermute x0 -> x15, waiting for transfers between devices: none -> 9.39 us  [the longest x8 7.54 us: collect_2(): lower.append(lax.ppermute(lower[-1] if lower else x, axis, pairs))]
  transfers between devices with their start and end apart: 3 -> 17, of which waited for: 2 -> 14; matrix products, arithmetic and copies ran while one was open for 2% -> 3% of each run, Pallas kernels for 0% -> 0%
where the time goes in v1:
time: 298 us; the launch traced here: 294 us
  waiting for transfers between devices  121 us (41%)
  starting transfers between devices  72.8 us (24%)
  blocking collectives  66.5 us (22%)
  between operations  13.7 us (5%)
  matrix products  7.77 us (3%)
  local copies, waits for them, and re-layouts  7.09 us (2%)
  other arithmetic  5.33 us (2%)
    all_gather x1, waiting for transfers between devices, side_by_side(): lax.all_gather(both, axis, axis=dim, tiled=True)  112 us
    all_to_all x1, blocking collectives, sent_and_summed(): parts = lax.all_to_all(cut_along(array, dim, count), axis, 0, 0, tiled=True)  66.5 us
    all_to_all x1, starting transfers between devices, from_everyone(): return lax.all_to_all(copies, axis, split_axis=0, concat_axis=0, tiled=True)  44.4 us
    ppermute x7, starting transfers between devices, collect_2(): upper.append(lax.ppermute(upper[-1] if upper else x, axis, back))  20.1 us
    ppermute x8, starting transfers between devices, collect_2(): lower.append(lax.ppermute(lower[-1] if lower else x, axis, pairs))  8.38 us
    ppermute x8, waiting for transfers between devices, collect_2(): lower.append(lax.ppermute(lower[-1] if lower else x, axis, pairs))  7.54 us
  transfers between devices with their start and end apart: 17, of which 14 were waited for; matrix products, arithmetic and copies ran while one was open for 3% of the time, Pallas kernels for 0%

profile of v1, /device:TPU:65, one launch (start us, length us, event | category | flops | bytes accessed | tf_op | source)
XLA Modules:
  0.0 294.4 jit_solution(11247523801610918864)
XLA Ops:
  6.6 0.9 convert_element_type.38
  7.5 0.9 convert_element_type.39
  9.2 0.9 convert_element_type.41
  10.1 1.3 broadcast_in_dim.2
  11.4 44.4 %all-to-all-start = ((bf16[16,352,128]{2,1,0:T(8,128)(2,1)}), bf16[16,352,128]{2,1,0:T(8,128)(2,1)}, u32[]{:S(2)}, u32[]{:S(2)}) async-start(bf16[16,352,128]{2,1,0:T(8,128)(2,1)} %broadcast_in_dim.2), calls=%async_computation | async-start | bytes 2883584 | tf_op jit(solution)/shard_map/all_to_all | solution.py:42
  56.3 111.8 %all-gather.2.cloned.1.call-done = bf16[2048,704]{0,1:T(8,128)(2,1)} async-done(((bf16[128,704]{0,1:T(8,128)(2,1)}), bf16[2048,704]{0,1:T(8,128)(2,1)}) %all-gather.2.cloned.1.call-update) | async-done | bytes 2883600 | tf_op jit(solution)/shard_map/all_gather | solution.py:37
  168.1 2.4 fusion.9
  170.5 5.4 %convolution_convert_fusion = bf16[512,2048]{1,0:T(8,128)(2,1)} fusion(bf16[2048,704]{0,1:T(8,128)(2,1)} %all-gather.2.cloned.1.call-done, f32[512,352]{0,1:T(8,128)S(1)} %fusion.9, bf16[512,2048]{1,0:T(8,128)(2,1)S(1)} %copy-done, f32[2048]{0:T(1024)S(1)} %copy-done.8, f32[512]{0:T(512)S(1)} %add_rsqrt_fusion, f32[352]{0:T(512)S(1)} %copy-done.10, ...), kind=kOutput, calls=%fused_computation.7 | convolution fusion | flops 1482899456 | bytes 7810432 | tf_op jit(solution)/shard_map/dot_general | solution.py:99
  175.9 66.5 %all_to_all.10 = bf16[16,32,2048]{2,1,0:T(8,128)(2,1)S(1)} all-to-all(bf16[16,32,2048]{2,1,0:T(8,128)(2,1)} %bitcast.52), channel_id=1, replica_groups=mesh['grp'=2,'fs'=16,'tp'=16] {'tp'}, dimensions={0} | all-to-all | bytes 4194304 | tf_op jit(solution)/shard_map/all_to_all | solution.py:64
  243.5 1.9 collective-permute-done
  245.4 2.4 collective-permute-start.1
  247.9 1.9 collective-permute-done.1
  249.8 2.4 collective-permute-start.2
  252.5 0.9 collective-permute-start.9
  254.3 2.3 collective-permute-start.3
  256.9 2.2 collective-permute-start.10
  259.9 1.1 collective-permute-start.4
  261.3 3.4 %collective-permute-start.11 = (bf16[32,2048]{1,0:T(8,128)(2,1)S(1)}, bf16[32,2048]{1,0:T(8,128)(2,1)S(1)}, u32[]{:S(2)}, u32[]{:S(2)}) collective-permute-start(bf16[32,2048]{1,0:T(8,128)(2,1)S(1)} %collective-permute-done.10), channel_id=1, source_target_pairs={{1,0},{2,1},{3,2},{4,3},{5,4},{6,5},{7,6},{8,7},{9,8},{10,9},{11,1... | collective-permute-start | bytes 393224 | tf_op jit(solution)/shard_map/ppermute | solution.py:24
  266.2 4.8 %collective-permute-start.12 = (bf16[32,2048]{1,0:T(8,128)(2,1)S(1)}, bf16[32,2048]{1,0:T(8,128)(2,1)S(1)}, u32[]{:S(2)}, u32[]{:S(2)}) collective-permute-start(bf16[32,2048]{1,0:T(8,128)(2,1)S(1)} %collective-permute-done.11), channel_id=1, source_target_pairs={{1,0},{2,1},{3,2},{4,3},{5,4},{6,5},{7,6},{8,7},{9,8},{10,9},{11,1... | collective-permute-start | bytes 393224 | tf_op jit(solution)/shard_map/ppermute | solution.py:24
  271.9 4.0 %collective-permute-start.13 = (bf16[32,2048]{1,0:T(8,128)(2,1)S(1)}, bf16[32,2048]{1,0:T(8,128)(2,1)S(1)}, u32[]{:S(2)}, u32[]{:S(2)}) collective-permute-start(bf16[32,2048]{1,0:T(8,128)(2,1)S(1)} %collective-permute-done.12), channel_id=1, source_target_pairs={{1,0},{2,1},{3,2},{4,3},{5,4},{6,5},{7,6},{8,7},{9,8},{10,9},{11,1... | collective-permute-start | bytes 393224 | tf_op jit(solution)/shard_map/ppermute | solution.py:24
  277.4 4.8 %collective-permute-start.14 = (bf16[32,2048]{1,0:T(8,128)(2,1)S(1)}, bf16[32,2048]{1,0:T(8,128)(2,1)S(1)}, u32[]{:S(2)}, u32[]{:S(2)}) collective-permute-start(bf16[32,2048]{1,0:T(8,128)(2,1)S(1)} %collective-permute-done.13), channel_id=1, source_target_pairs={{1,0},{2,1},{3,2},{4,3},{5,4},{6,5},{7,6},{8,7},{9,8},{10,9},{11,1... | collective-permute-start | bytes 393224 | tf_op jit(solution)/shard_map/ppermute | solution.py:24
  282.4 0.9 bitcast_dynamic-update-slice_fusion.13
  283.3 0.9 bitcast_dynamic-update-slice_fusion.12
  285.4 2.1 gather_fusion
  (66 shorter events, 10.1 us)
Async XLA Ops:
  6.5 161.6 %all-gather.2.cloned.1.call-start = ((), (), s32[]{:S(2)}) async-start(), calls=%async_computation.2 | async-start | bytes 3063808 | tf_op jit(solution)/shard_map/all_gather | solution.py:37
  10.1 45.7 %copy-start = (bf16[512,2048]{1,0:T(8,128)(2,1)S(1)}, bf16[512,2048]{1,0:T(8,128)(2,1)}, u32[]{:S(2)}) copy-start(bf16[512,2048]{1,0:T(8,128)(2,1)} %param.9) | copy-start | bytes 6291460
  11.4 156.7 %copy-start.8 = (f32[2048]{0:T(1024)S(1)}, f32[2048]{0:T(1024)}, u32[]{:S(2)}) copy-start(f32[2048]{0:T(1024)} %param.10) | copy-start | bytes 24580
  11.4 156.7 %copy-start.9 = (f32[352]{0:T(512)S(1)}, f32[352]{0:T(512)}, u32[]{:S(2)}) copy-start(f32[352]{0:T(512)} %param.12) | copy-start | bytes 4228
  11.4 159.1 %all-to-all-start = ((bf16[16,352,128]{2,1,0:T(8,128)(2,1)}), bf16[16,352,128]{2,1,0:T(8,128)(2,1)}, u32[]{:S(2)}, u32[]{:S(2)}) async-start(bf16[16,352,128]{2,1,0:T(8,128)(2,1)} %broadcast_in_dim.2), calls=%async_computation | async-start | bytes 2883584 | tf_op jit(solution)/shard_map/all_to_all | solution.py:42
  56.3 114.2 %copy-start.10 = (f32[352]{0:T(512)S(1)}, f32[352]{0:T(512)}, u32[]{:S(2)}) copy-start(f32[352]{0:T(512)} %param.14) | copy-start | bytes 4228
  243.4 2.0 collective-permute-start
  245.4 4.4 %collective-permute-start.1 = (bf16[32,2048]{1,0:T(8,128)(2,1)S(1)}, bf16[32,2048]{1,0:T(8,128)(2,1)S(1)}, u32[]{:S(2)}, u32[]{:S(2)}) collective-permute-start(bf16[32,2048]{1,0:T(8,128)(2,1)S(1)} %collective-permute-done), channel_id=1, source_target_pairs={{0,1},{1,2},{2,3},{3,4},{4,5},{5,6},{6,7},{7,8},{8,9},{9,10},{10,1... | collective-permute-start | bytes 393224 | tf_op jit(solution)/shard_map/ppermute | solution.py:22
  247.9 4.7 %collective-permute-start.8 = (bf16[32,2048]{1,0:T(8,128)(2,1)S(1)}, bf16[32,2048]{1,0:T(8,128)(2,1)S(1)}, u32[]{:S(2)}, u32[]{:S(2)}) collective-permute-start(bf16[32,2048]{1,0:T(8,128)(2,1)S(1)} %multiply_convert_fusion), channel_id=1, source_target_pairs={{1,0},{2,1},{3,2},{4,3},{5,4},{6,5},{7,6},{8,7},{9,8},{10,9},{11,1... | collective-permute-start | bytes 393224 | tf_op jit(solution)/shard_map/ppermute | solution.py:24
  249.8 4.5 %collective-permute-start.2 = (bf16[32,2048]{1,0:T(8,128)(2,1)S(1)}, bf16[32,2048]{1,0:T(8,128)(2,1)S(1)}, u32[]{:S(2)}, u32[]{:S(2)}) collective-permute-start(bf16[32,2048]{1,0:T(8,128)(2,1)S(1)} %collective-permute-done.1), channel_id=1, source_target_pairs={{0,1},{1,2},{2,3},{3,4},{4,5},{5,6},{6,7},{7,8},{8,9},{9,10},{10,1... | collective-permute-start | bytes 393224 | tf_op jit(solution)/shard_map/ppermute | solution.py:22
  252.5 4.4 %collective-permute-start.9 = (bf16[32,2048]{1,0:T(8,128)(2,1)S(1)}, bf16[32,2048]{1,0:T(8,128)(2,1)S(1)}, u32[]{:S(2)}, u32[]{:S(2)}) collective-permute-start(bf16[32,2048]{1,0:T(8,128)(2,1)S(1)} %collective-permute-done.8), channel_id=1, source_target_pairs={{1,0},{2,1},{3,2},{4,3},{5,4},{6,5},{7,6},{8,7},{9,8},{10,9},{11,1... | collective-permute-start | bytes 393224 | tf_op jit(solution)/shard_map/ppermute | solution.py:24
  254.3 5.6 %collective-permute-start.3 = (bf16[32,2048]{1,0:T(8,128)(2,1)S(1)}, bf16[32,2048]{1,0:T(8,128)(2,1)S(1)}, u32[]{:S(2)}, u32[]{:S(2)}) collective-permute-start(bf16[32,2048]{1,0:T(8,128)(2,1)S(1)} %collective-permute-done.2), channel_id=1, source_target_pairs={{0,1},{1,2},{2,3},{3,4},{4,5},{5,6},{6,7},{7,8},{8,9},{9,10},{10,1... | collective-permute-start | bytes 393224 | tf_op jit(solution)/shard_map/ppermute | solution.py:22
  256.9 4.4 %collective-permute-start.10 = (bf16[32,2048]{1,0:T(8,128)(2,1)S(1)}, bf16[32,2048]{1,0:T(8,128)(2,1)S(1)}, u32[]{:S(2)}, u32[]{:S(2)}) collective-permute-start(bf16[32,2048]{1,0:T(8,128)(2,1)S(1)} %collective-permute-done.9), channel_id=1, source_target_pairs={{1,0},{2,1},{3,2},{4,3},{5,4},{6,5},{7,6},{8,7},{9,8},{10,9},{11,1... | collective-permute-start | bytes 393224 | tf_op jit(solution)/shard_map/ppermute | solution.py:24
  259.9 5.6 %collective-permute-start.4 = (bf16[32,2048]{1,0:T(8,128)(2,1)S(1)}, bf16[32,2048]{1,0:T(8,128)(2,1)S(1)}, u32[]{:S(2)}, u32[]{:S(2)}) collective-permute-start(bf16[32,2048]{1,0:T(8,128)(2,1)S(1)} %collective-permute-done.3), channel_id=1, source_target_pairs={{0,1},{1,2},{2,3},{3,4},{4,5},{5,6},{6,7},{7,8},{8,9},{9,10},{10,1... | collective-permute-start | bytes 393224 | tf_op jit(solution)/shard_map/ppermute | solution.py:22
  261.3 4.4 %collective-permute-start.11 = (bf16[32,2048]{1,0:T(8,128)(2,1)S(1)}, bf16[32,2048]{1,0:T(8,128)(2,1)S(1)}, u32[]{:S(2)}, u32[]{:S(2)}) collective-permute-start(bf16[32,2048]{1,0:T(8,128)(2,1)S(1)} %collective-permute-done.10), channel_id=1, source_target_pairs={{1,0},{2,1},{3,2},{4,3},{5,4},{6,5},{7,6},{8,7},{9,8},{10,9},{11,1... | collective-permute-start | bytes 393224 | tf_op jit(solution)/shard_map/ppermute | solution.py:24
  265.5 5.6 %collective-permute-start.5 = (bf16[32,2048]{1,0:T(8,128)(2,1)S(1)}, bf16[32,2048]{1,0:T(8,128)(2,1)S(1)}, u32[]{:S(2)}, u32[]{:S(2)}) collective-permute-start(bf16[32,2048]{1,0:T(8,128)(2,1)S(1)} %collective-permute-done.4), channel_id=1, source_target_pairs={{0,1},{1,2},{2,3},{3,4},{4,5},{5,6},{6,7},{7,8},{8,9},{9,10},{10,1... | collective-permute-start | bytes 393224 | tf_op jit(solution)/shard_map/ppermute | solution.py:22
  266.2 5.7 %collective-permute-start.12 = (bf16[32,2048]{1,0:T(8,128)(2,1)S(1)}, bf16[32,2048]{1,0:T(8,128)(2,1)S(1)}, u32[]{:S(2)}, u32[]{:S(2)}) collective-permute-start(bf16[32,2048]{1,0:T(8,128)(2,1)S(1)} %collective-permute-done.11), channel_id=1, source_target_pairs={{1,0},{2,1},{3,2},{4,3},{5,4},{6,5},{7,6},{8,7},{9,8},{10,9},{11,1... | collective-permute-start | bytes 393224 | tf_op jit(solution)/shard_map/ppermute | solution.py:24
  271.1 11.0 %copy-start.2 = (bf16[32,2048]{1,0:T(8,128)(2,1)}, bf16[32,2048]{1,0:T(8,128)(2,1)S(1)}, u32[]{:S(2)}) copy-start(bf16[32,2048]{1,0:T(8,128)(2,1)S(1)} %collective-permute-done.5) | copy-start | bytes 393220
  271.1 5.6 %collective-permute-start.6 = (bf16[32,2048]{1,0:T(8,128)(2,1)S(1)}, bf16[32,2048]{1,0:T(8,128)(2,1)S(1)}, u32[]{:S(2)}, u32[]{:S(2)}) collective-permute-start(bf16[32,2048]{1,0:T(8,128)(2,1)S(1)} %collective-permute-done.5), channel_id=1, source_target_pairs={{0,1},{1,2},{2,3},{3,4},{4,5},{5,6},{6,7},{7,8},{8,9},{9,10},{10,1... | collective-permute-start | bytes 393224 | tf_op jit(solution)/shard_map/ppermute | solution.py:22
  271.1 14.1 %copy-start.7 = (f32[32]{0:T(128)S(1)}, f32[32]{0:T(128)}, u32[]{:S(2)}) copy-start(f32[32]{0:T(128)} %copy-done.6) | copy-start | bytes 388
  271.9 5.4 %collective-permute-start.13 = (bf16[32,2048]{1,0:T(8,128)(2,1)S(1)}, bf16[32,2048]{1,0:T(8,128)(2,1)S(1)}, u32[]{:S(2)}, u32[]{:S(2)}) collective-permute-start(bf16[32,2048]{1,0:T(8,128)(2,1)S(1)} %collective-permute-done.12), channel_id=1, source_target_pairs={{1,0},{2,1},{3,2},{4,3},{5,4},{6,5},{7,6},{8,7},{9,8},{10,9},{11,1... | collective-permute-start | bytes 393224 | tf_op jit(solution)/shard_map/ppermute | solution.py:24
  276.7 5.4 %copy-start.3 = (bf16[32,2048]{1,0:T(8,128)(2,1)}, bf16[32,2048]{1,0:T(8,128)(2,1)S(1)}, u32[]{:S(2)}) copy-start(bf16[32,2048]{1,0:T(8,128)(2,1)S(1)} %collective-permute-done.6) | copy-start | bytes 393220
  276.7 5.6 %collective-permute-start.7 = (bf16[32,2048]{1,0:T(8,128)(2,1)S(1)}, bf16[32,2048]{1,0:T(8,128)(2,1)S(1)}, u32[]{:S(2)}, u32[]{:S(2)}) collective-permute-start(bf16[32,2048]{1,0:T(8,128)(2,1)S(1)} %collective-permute-done.6), channel_id=1, source_target_pairs={{0,1},{1,2},{2,3},{3,4},{4,5},{5,6},{6,7},{7,8},{8,9},{9,10},{10,1... | collective-permute-start | bytes 393224 | tf_op jit(solution)/shard_map/ppermute | solution.py:22
  277.4 8.0 %collective-permute-start.14 = (bf16[32,2048]{1,0:T(8,128)(2,1)S(1)}, bf16[32,2048]{1,0:T(8,128)(2,1)S(1)}, u32[]{:S(2)}, u32[]{:S(2)}) collective-permute-start(bf16[32,2048]{1,0:T(8,128)(2,1)S(1)} %collective-permute-done.13), channel_id=1, source_target_pairs={{1,0},{2,1},{3,2},{4,3},{5,4},{6,5},{7,6},{8,7},{9,8},{10,9},{11,1... | collective-permute-start | bytes 393224 | tf_op jit(solution)/shard_map/ppermute | solution.py:24
  (4 other events, 6.8 us)
Sparse Core Ops, SparseCore 0:
  9.4 158.6 all-gather.1
